TPU v7x, 512 devices: a whole 4x4x16 slice. The times are simulated.
512 devices in a mesh: gr: 2 (over z_hi), fs: 32 (over z_lo, y), tp: 8 (over x, core).
Axes of the slice: x: 4, y: 4, z: 16 (z_hi: 2, z_lo: 8; z = z_hi * 8 + z_lo), core: 2. Of those that a mesh axis runs over, the one named last changes fastest.
Arguments:
- tokens: bfloat16 [8192, 2048], P(('gr', 'fs')), may hold values from -60 to 60
- route_ids: int32 [8192, 2], P(('gr', 'fs')), may hold values from 0 to 7, all different within a row; in each aligned block of 128 rows (0 to 127, 128 to 255, ...) at most 32 rows name the same one
- route_logits: float32 [8192, 2], P(('gr', 'fs')), may hold values from -8 to 8
- norm_gain: float32 [2048], P(('gr', 'fs')), may hold values from 0.1 to 1.9
- gate_master: float32 [8, 2048, 7168], P(None, ('gr', 'fs'), 'tp'), may hold values from -0.125 to 0.125
- up_master: float32 [8, 2048, 7168], P(None, ('gr', 'fs'), 'tp'), may hold values from -0.125 to 0.125
- down_master: float32 [8, 7168, 2048], P(None, 'fs', ('gr', 'tp')), may hold values from -0.0625 to 0.0625
Outputs:
- gate_weight: bfloat16 [8, 2048, 7168], P('tp', None, 'fs')
- up_weight: bfloat16 [8, 2048, 7168], P('tp', None, 'fs')
- down_weight: bfloat16 [8, 7168, 2048], P('tp', 'fs')
- mixed: bfloat16 [8192, 2048], P(('gr', 'fs'))
Inputs may be any that keep to these rules, and one draw needn't show every extreme that they name: `route_ids`: in the rows of one device, that is in each aligned block of 128 rows, each of the 8 experts is named by exactly 32 rows; a row names two different experts.
All inputs are finite; a program needn't handle non-finite values.
Results may differ from a plain program's by a relative error of at most 0.025.
Values may be sent and summed in bfloat16 or wider, within the bound.
No kernel may reach another device: no remote copies, remote signals or barrier semaphores. Data moves between devices by JAX's collectives and lax.ppermute only.
A program may use at most 64 MiB of HBM per device.

v0:
```python
import jax
import jax.numpy as jnp
from jax import lax
from jax.experimental import pallas as pl
from jax.experimental.pallas import tpu as pltpu
from jax.sharding import Mesh
from jax.sharding import PartitionSpec as P


CAP = 32
FS = ("fs_0", "fs_1")
GR_FS = ("gr", "fs_0", "fs_1")
ALL = ("gr", "fs_0", "fs_1", "tp")
EPS = 1e-06
LANES = 128


def lane_window(blocks, start):
    first, offset = divmod(start, LANES)
    if offset == 0:
        return blocks[first]
    head = pltpu.roll(blocks[first], LANES - offset, 1)
    if first + 1 == len(blocks):
        return head
    rest = pltpu.roll(blocks[first + 1], LANES - offset, 1)
    lane = lax.broadcasted_iota(jnp.int32, head.shape, 1)
    return jnp.where(lane < LANES - offset, head, rest)


def pack_kernel(gate_ref, up_ref, gain_ref, out_ref):
    gain = gain_ref[...]
    both = jnp.concatenate([gate_ref[0] * gain, up_ref[0] * gain], axis=0)
    blocks = [both[:, LANES * b : LANES * (b + 1)] for b in range(both.shape[1] // LANES)]
    lane = lax.broadcasted_iota(jnp.int32, (48, LANES), 1)
    for j in range(4):
        main = lane_window(blocks, 224 * j)
        tail = lane_window(blocks, 224 * j + LANES)
        last = tail[48:]
        spread = jnp.concatenate([pltpu.roll(last, 96 - 32 * q, 1) for q in range(3)], axis=0)
        out_ref[0, j, :64, :] = main.astype(jnp.bfloat16)
        out_ref[0, j, 64:, :] = jnp.where(lane < 96, tail[:48], spread).astype(jnp.bfloat16)


def pack(gate_master, up_master, gain):
    experts, rows, cols = gate_master.shape
    return pl.pallas_call(
        pack_kernel,
        grid=(experts,),
        in_specs=[
            pl.BlockSpec((1, rows, cols), lambda i: (i, 0, 0)),
            pl.BlockSpec((1, rows, cols), lambda i: (i, 0, 0)),
            pl.BlockSpec((rows, 1), lambda i: (0, 0)),
        ],
        out_specs=pl.BlockSpec((1, 4, 112, LANES), lambda i: (i, 0, 0, 0)),
        out_shape=jax.ShapeDtypeStruct((experts, 4, 112, LANES), jnp.bfloat16),
        cost_estimate=pl.CostEstimate(flops=4000000, bytes_accessed=2800000, transcendentals=0),
        compiler_params=pltpu.CompilerParams(vmem_limit_bytes=4 * 2**20),
        name="pack",
    )(gate_master, up_master, gain)


def unpack_kernel(tiles_ref, gate_ref, up_ref):
    lane = lax.broadcasted_iota(jnp.int32, (16, LANES), 1)
    for s in range(tiles_ref.shape[0]):
        rows = pl.ds(32 * s, 32)
        gate_ref[0, rows, :LANES] = tiles_ref[s, 0:32, :]
        up_ref[0, rows, :LANES] = tiles_ref[s, 32:64, :]
        gate_ref[0, rows, LANES:] = tiles_ref[s, 64:96, :96]
        up_ref[0, pl.ds(32 * s, 16), LANES:] = tiles_ref[s, 96:112, :96]
        parts = [
            pltpu.roll(
                tiles_ref[s, 64 + 16 * q : 80 + 16 * q, :].astype(jnp.float32), 32 * q + 32, 1
            )
            for q in range(3)
        ]
        last = jnp.where(lane < 32, parts[0], jnp.where(lane < 64, parts[1], parts[2]))
        up_ref[0, pl.ds(32 * s + 16, 16), LANES:] = last[:, :96].astype(jnp.bfloat16)


def unpack(tiles):
    count = tiles.shape[0]
    step = 16
    out = jax.ShapeDtypeStruct((1, 32 * count, 224), jnp.bfloat16)
    return pl.pallas_call(
        unpack_kernel,
        grid=(count // step,),
        in_specs=[pl.BlockSpec((step, 112, LANES), lambda i: (i, 0, 0))],
        out_specs=[pl.BlockSpec((1, 32 * step, 224), lambda i: (0, i, 0))] * 2,
        out_shape=[out, out],
        cost_estimate=pl.CostEstimate(flops=2000000, bytes_accessed=3800000, transcendentals=0),
        compiler_params=pltpu.CompilerParams(vmem_limit_bytes=6 * 2**20),
        name="unpack",
    )(tiles)


def permutation(sizes, move):
    groups, fs_0, fs_1, tp = sizes
    pairs = []
    for g in range(groups):
        for a in range(fs_0):
            for b in range(fs_1):
                for t in range(tp):
                    z, y = move(g * fs_0 + a, b, t)
                    z, y = z % (groups * fs_0), y % fs_1
                    pairs.append((((g * fs_0 + a) * fs_1 + b) * tp + t, (z * fs_1 + y) * tp + t))
    return pairs


def local(sizes, tokens, route_ids, route_logits, norm_gain, gate_master, up_master, down_master):
    f32, bf16 = jnp.float32, jnp.bfloat16
    fs_1, tp_size = sizes[2], sizes[3]

    def along_z(x, hops):
        pairs = permutation(sizes, lambda z, y, t: (z + (hops if t % 2 == 0 else -hops), y))
        return lax.ppermute(x, ALL, pairs)

    def along_y(x, hops):
        return lax.ppermute(x, ALL, permutation(sizes, lambda z, y, t: (z, y + hops)))

    as_float = tokens.astype(f32)
    normed = (
        as_float * lax.rsqrt(jnp.mean(as_float * as_float, axis=-1, keepdims=True) + EPS)
    ).astype(bf16)
    differ = route_logits[:, 0] - route_logits[:, 1]
    route_weight = jnp.stack([jax.nn.sigmoid(differ), jax.nn.sigmoid(-differ)], axis=1)
    expert_ids = jnp.arange(tp_size, dtype=jnp.int32)
    route_hits = route_ids[None, :, :] == expert_ids[:, None, None]
    chosen = jnp.any(route_hits, axis=2)
    slot_rank = jnp.cumsum(chosen.astype(jnp.int32), axis=1) - 1
    slot_ids = jnp.arange(CAP, dtype=jnp.int32)
    picker = chosen[:, None, :] & (slot_rank[:, None, :] == slot_ids[None, :, None])
    weight_rows = jnp.sum(jnp.where(route_hits, route_weight[None, :, :], 0.0), axis=2)
    mine = lax.axis_index("tp")
    my_picker = lax.dynamic_index_in_dim(picker, mine, 0, keepdims=False)
    my_weights = lax.dynamic_index_in_dim(weight_rows, mine, 0, keepdims=False)
    slot_weight = jnp.sum(jnp.where(my_picker, my_weights[None, :], 0.0), axis=1)
    packed = jnp.dot(my_picker.astype(bf16), normed, preferred_element_type=f32).astype(bf16)

    down_half = down_master.astype(bf16)
    down_tiles = lax.all_to_all(down_half, "tp", 0, 0, tiled=True)
    down_own = jnp.moveaxis(down_tiles, 0, 1).reshape(down_tiles.shape[1], -1)
    across = permutation(sizes, lambda z, y, t: (z + sizes[1], y))
    down_other = lax.ppermute(down_own, ALL, across)

    tiles = pack(gate_master, up_master, norm_gain[:, None])
    tiles = lax.all_to_all(tiles, "tp", 0, 0, tiled=True).reshape(-1, 112, LANES)
    tiles = jnp.concatenate([tiles, tiles], axis=0)
    tiles = lax.all_to_all(tiles, GR_FS, 0, 0, tiled=True)

    held = packed
    for hops in (4, 2, 1):
        moved = along_z(held, hops)
        held = jnp.concatenate([held, moved], axis=0)
    row = lax.axis_index("fs_1")
    gathered = jnp.zeros((fs_1, *held.shape), bf16)
    for k in range(fs_1):
        moved = held
        if k:
            moved = along_y(held, k)
        gathered = lax.dynamic_update_index_in_dim(gathered, moved, (row + fs_1 - k) % fs_1, 0)
    gathered = gathered.reshape(-1, gathered.shape[2])
    tiles, gathered, down_other = lax.optimization_barrier((tiles, gathered, down_other))

    gate_weight, up_weight = unpack(tiles)
    low = lax.axis_index("gr") == 0
    down_parts = [jnp.where(low, down_own, down_other), jnp.where(low, down_other, down_own)]
    down_weight = jnp.concatenate(down_parts, axis=1)[None]

    gate_act = jnp.dot(gathered, gate_weight[0], preferred_element_type=f32)
    up_act = jnp.dot(gathered, up_weight[0], preferred_element_type=f32)
    hidden = (jax.nn.silu(gate_act) * up_act).astype(bf16)
    everyone = picker.reshape(-1, picker.shape[2]).astype(bf16)
    mixed = []
    for part in down_parts:
        sums = jnp.dot(hidden, part, preferred_element_type=f32).astype(bf16)
        sums = lax.all_to_all(sums.reshape(fs_1, -1, sums.shape[1]), "fs_1", 0, 0, tiled=True)
        total = jnp.sum(sums.astype(f32), axis=0)
        for hops in (1, 2, 4):
            half = total.shape[0] // 2
            moved = along_z(total[half:].astype(bf16), -hops)
            total = total[:half] + moved.astype(f32)
        block = (total * slot_weight[:, None]).astype(bf16)
        block, slot_weight = lax.optimization_barrier((block, slot_weight))
        blocks = lax.all_to_all(
            jnp.broadcast_to(block[None], (tp_size, *block.shape)), "tp", 0, 0, tiled=True
        )
        mixed.append(
            lax.dot_general(
                everyone,
                blocks.reshape(-1, blocks.shape[2]),
                (((0,), (0,)), ((), ())),
                preferred_element_type=f32,
            ).astype(bf16)
        )
    return (gate_weight, up_weight, down_weight, jnp.concatenate(mixed, axis=1))


def solution(mesh):
    sizes = (mesh.shape["gr"], 8, 4, mesh.shape["tp"])
    torus = Mesh(mesh.devices.reshape(sizes), ALL)
    in_specs = (
        P(GR_FS, None),
        P(GR_FS, None),
        P(GR_FS, None),
        P(GR_FS),
        P(None, GR_FS, "tp"),
        P(None, GR_FS, "tp"),
        P(None, FS, ("gr", "tp")),
    )
    out_specs = (P("tp", None, FS), P("tp", None, FS), P("tp", FS, None), P(GR_FS, None))

    def call(*arrays):
        return local(sizes, *arrays)

    return jax.shard_map(call, mesh=torus, in_specs=in_specs, out_specs=out_specs, check_vma=False)
```

profile of v0, /device:TPU:1, one launch (start us, length us, event | category | flops | bytes accessed | tf_op | source)
XLA Modules:
  0.0 360.8 jit_solution(15496983183100415822)
XLA Ops:
  1.4 1.2 copy-done.2
  3.7 3.7 %pack.1 = bf16[8,4,112,128]{3,2,1,0:T(8,128)(2,1)} custom-call(f32[8,32,896]{2,1,0:T(8,128)S(1)} %copy-done.2, f32[8,32,896]{2,1,0:T(8,128)S(1)} %copy-done.3, f32[32,1]{1,0:T(8,128)S(1)} %copy.17.gain_ref), custom_call_target="tpu_custom_call" | custom-call | flops 4000000 | bytes 2800000 | tf_op jit(solution)/shard_map/pack/pallas_call | solution.py:46
  7.5 10.4 %all-to-all-start = ((bf16[8,4,112,128]{3,2,1,0:T(8,128)(2,1)}), bf16[8,4,112,128]{3,2,1,0:T(8,128)(2,1)S(1)}, u32[]{:S(2)}, u32[]{:S(2)}) async-start(bf16[8,4,112,128]{3,2,1,0:T(8,128)(2,1)} %pack.1), calls=%async_computation | async-start | bytes 1835008 | tf_op jit(solution)/shard_map/all_to_all | solution.py:146
  18.7 12.8 %all-to-all-done = bf16[8,4,112,128]{3,2,1,0:T(8,128)(2,1)S(1)} async-done(((bf16[8,4,112,128]{3,2,1,0:T(8,128)(2,1)}), bf16[8,4,112,128]{3,2,1,0:T(8,128)(2,1)S(1)}, u32[]{:S(2)}, u32[]{:S(2)}) %all-to-all-start) | async-done | bytes 917536 | tf_op jit(solution)/shard_map/all_to_all | solution.py:146
  31.5 4.3 %all-to-all-start.2 = ((bf16[8,224,128]{2,1,0:T(8,128)(2,1)}), bf16[8,224,128]{2,1,0:T(8,128)(2,1)S(1)}, u32[]{:S(2)}, u32[]{:S(2)}) async-start(bf16[8,224,128]{2,1,0:T(8,128)(2,1)} %convert_element_type.76), calls=%async_computation.2 | async-start | bytes 917504 | tf_op jit(solution)/shard_map/all_to_all | solution.py:140
  35.8 1.4 pad_maximum_fusion
  37.3 7.3 %all-to-all-done.2 = bf16[8,224,128]{2,1,0:T(8,128)(2,1)S(1)} async-done(((bf16[8,224,128]{2,1,0:T(8,128)(2,1)}), bf16[8,224,128]{2,1,0:T(8,128)(2,1)S(1)}, u32[]{:S(2)}, u32[]{:S(2)}) %all-to-all-start.2) | async-done | bytes 458784 | tf_op jit(solution)/shard_map/all_to_all | solution.py:140
  44.5 13.9 %all-to-all-start.1 = ((bf16[64,112,128]{2,1,0:T(8,128)(2,1)}), bf16[64,112,128]{2,1,0:T(8,128)(2,1)S(1)}, u32[]{:S(2)}, u32[]{:S(2)}) async-start(bf16[64,112,128]{2,1,0:T(8,128)(2,1)} %pad_maximum_fusion), calls=%async_computation.1 | async-start | bytes 3670016 | tf_op jit(solution)/shard_map/all_to_all | solution.py:148
  59.3 7.0 %collective-permute-start = (bf16[32,2048]{1,0:T(8,128)(2,1)S(1)}, bf16[32,2048]{1,0:T(8,128)(2,1)S(1)}, u32[]{:S(2)}, u32[]{:S(2)}) collective-permute-start(bf16[32,2048]{1,0:T(8,128)(2,1)S(1)} %convolution_convert_fusion), channel_id=1, source_target_pairs={{0,128},{1,385},{2,130},{3,387},{4,132},{5,389},{6,134},{7,391},{8... | collective-permute-start | bytes 393224 | tf_op jit(solution)/shard_map/ppermute | solution.py:115
  66.3 81.2 %collective-permute-done = bf16[32,2048]{1,0:T(8,128)(2,1)S(1)} collective-permute-done((bf16[32,2048]{1,0:T(8,128)(2,1)S(1)}, bf16[32,2048]{1,0:T(8,128)(2,1)S(1)}, u32[]{:S(2)}, u32[]{:S(2)}) %collective-permute-start) | collective-permute-done | bytes 131104 | tf_op jit(solution)/shard_map/ppermute | solution.py:115
  147.5 1.9 collective-permute-start.1
  149.5 7.4 %collective-permute-done.1 = bf16[64,2048]{1,0:T(8,128)(2,1)S(1)} collective-permute-done((bf16[64,2048]{1,0:T(8,128)(2,1)S(1)}, bf16[64,2048]{1,0:T(8,128)(2,1)S(1)}, u32[]{:S(2)}, u32[]{:S(2)}) %collective-permute-start.1) | collective-permute-done | bytes 262176 | tf_op jit(solution)/shard_map/ppermute | solution.py:115
  156.9 4.2 %collective-permute-start.2 = (bf16[128,2048]{1,0:T(8,128)(2,1)S(1)}, bf16[128,2048]{1,0:T(8,128)(2,1)S(1)}, u32[]{:S(2)}, u32[]{:S(2)}) collective-permute-start(bf16[128,2048]{1,0:T(8,128)(2,1)S(1)} %pad_maximum_fusion.2), channel_id=1, source_target_pairs={{0,32},{1,481},{2,34},{3,483},{4,36},{5,485},{6,38},{7,487},{8,40}... | collective-permute-start | bytes 1572872 | tf_op jit(solution)/shard_map/ppermute | solution.py:115
  161.1 7.1 %collective-permute-done.2 = bf16[128,2048]{1,0:T(8,128)(2,1)S(1)} collective-permute-done((bf16[128,2048]{1,0:T(8,128)(2,1)S(1)}, bf16[128,2048]{1,0:T(8,128)(2,1)S(1)}, u32[]{:S(2)}, u32[]{:S(2)}) %collective-permute-start.2) | collective-permute-done | bytes 524320 | tf_op jit(solution)/shard_map/ppermute | solution.py:115
  169.2 3.0 collective-permute-start.3
  172.2 5.3 %collective-permute-start.4 = (bf16[256,2048]{1,0:T(8,128)(2,1)}, bf16[256,2048]{1,0:T(8,128)(2,1)}, u32[]{:S(2)}, u32[]{:S(2)}) collective-permute-start(bf16[256,2048]{1,0:T(8,128)(2,1)} %pad_maximum_fusion.1), channel_id=1, source_target_pairs={{0,16},{1,17},{2,18},{3,19},{4,20},{5,21},{6,22},{7,23},{8,24},{9,... | collective-permute-start | bytes 3145736 | tf_op jit(solution)/shard_map/ppermute | solution.py:118
  177.7 8.0 %collective-permute-start.6 = (bf16[224,1024]{1,0:T(8,128)(2,1)S(1)}, bf16[224,1024]{1,0:T(8,128)(2,1)}, u32[]{:S(2)}, u32[]{:S(2)}) collective-permute-start(bf16[224,1024]{1,0:T(8,128)(2,1)S(1)} %copy_bitcast_fusion), channel_id=1, source_target_pairs={{0,256},{1,257},{2,258},{3,259},{4,260},{5,261},{6,262},{7,263},{8... | collective-permute-start | bytes 1376264 | tf_op jit(solution)/shard_map/ppermute | solution.py:143
  185.7 1.9 collective-permute-start.5
  188.3 5.2 %collective-permute-done.3 = bf16[256,2048]{1,0:T(8,128)(2,1)} collective-permute-done((bf16[256,2048]{1,0:T(8,128)(2,1)}, bf16[256,2048]{1,0:T(8,128)(2,1)}, u32[]{:S(2)}, u32[]{:S(2)}) %collective-permute-start.3) | collective-permute-done | bytes 1048608 | tf_op jit(solution)/shard_map/ppermute | solution.py:118
  193.5 1.3 bitcast_dynamic-update-slice_fusion.2
  194.8 22.5 %collective-permute-done.4 = bf16[256,2048]{1,0:T(8,128)(2,1)} collective-permute-done((bf16[256,2048]{1,0:T(8,128)(2,1)}, bf16[256,2048]{1,0:T(8,128)(2,1)}, u32[]{:S(2)}, u32[]{:S(2)}) %collective-permute-start.4) | collective-permute-done | bytes 1048608 | tf_op jit(solution)/shard_map/ppermute | solution.py:118
  217.3 1.3 bitcast_dynamic-update-slice_fusion.1
  218.7 3.7 %collective-permute-done.5 = bf16[256,2048]{1,0:T(8,128)(2,1)S(1)} collective-permute-done((bf16[256,2048]{1,0:T(8,128)(2,1)}, bf16[256,2048]{1,0:T(8,128)(2,1)S(1)}, u32[]{:S(2)}, u32[]{:S(2)}) %collective-permute-start.5) | collective-permute-done | bytes 1048608 | tf_op jit(solution)/shard_map/ppermute | solution.py:118
  222.5 2.0 copy-done.4
  225.1 4.1 %fusion.6 = f32[1024,224]{0,1:T(8,128)S(1)} fusion(bf16[1024,2048]{1,0:T(8,128)(2,1)} %bitcast.59, bf16[1,2048,224]{2,1,0:T(8,128)(2,1)S(1)} %get-tuple-element.24), kind=kOutput, calls=%fused_computation.17 | convolution fusion | flops 939524096 | bytes 6029312 | tf_op jit(solution)/shard_map/dot_general | solution.py:169
  229.2 1.5 multiply_convert_fusion
  230.8 1.2 broadcast_select_fusion.1
  232.0 2.1 convolution_convert_fusion.2
  234.1 4.6 %all-to-all-start.3 = ((bf16[4,256,1024]{2,1,0:T(8,128)(2,1)}), bf16[4,256,1024]{2,1,0:T(8,128)(2,1)}, u32[]{:S(2)}, u32[]{:S(2)}) async-start(bf16[4,256,1024]{2,1,0:T(8,128)(2,1)} %bitcast.58), calls=%async_computation.3 | async-start | bytes 4194304 | tf_op jit(solution)/shard_map/all_to_all | solution.py:176
  238.7 2.1 convolution_convert_fusion.1
  240.8 22.7 %all-to-all-done.3 = bf16[4,256,1024]{2,1,0:T(8,128)(2,1)} async-done(((bf16[4,256,1024]{2,1,0:T(8,128)(2,1)}), bf16[4,256,1024]{2,1,0:T(8,128)(2,1)}, u32[]{:S(2)}, u32[]{:S(2)}) %all-to-all-start.3) | async-done | bytes 2097184 | tf_op jit(solution)/shard_map/all_to_all | solution.py:176
  263.5 4.6 %all-to-all-start.5 = ((bf16[4,256,1024]{2,1,0:T(8,128)(2,1)}), bf16[4,256,1024]{2,1,0:T(8,128)(2,1)}, u32[]{:S(2)}, u32[]{:S(2)}) async-start(bf16[4,256,1024]{2,1,0:T(8,128)(2,1)} %bitcast.57), calls=%async_computation.5 | async-start | bytes 4194304 | tf_op jit(solution)/shard_map/all_to_all | solution.py:176
  268.2 2.1 convert_reduce_fusion.1
  270.3 4.1 %collective-permute-start.7 = (bf16[128,1024]{1,0:T(8,128)(2,1)S(1)}, bf16[128,1024]{1,0:T(8,128)(2,1)S(1)}, u32[]{:S(2)}, u32[]{:S(2)}) collective-permute-start(bf16[128,1024]{1,0:T(8,128)(2,1)S(1)} %slice.105), channel_id=1, source_target_pairs={{0,480},{1,33},{2,482},{3,35},{4,484},{5,37},{6,486},{7,39},{8,488... | collective-permute-start | bytes 786440 | tf_op jit(solution)/shard_map/ppermute | solution.py:115
  274.4 17.5 %all-to-all-done.5 = bf16[4,256,1024]{2,1,0:T(8,128)(2,1)} async-done(((bf16[4,256,1024]{2,1,0:T(8,128)(2,1)}), bf16[4,256,1024]{2,1,0:T(8,128)(2,1)}, u32[]{:S(2)}, u32[]{:S(2)}) %all-to-all-start.5) | async-done | bytes 2097184 | tf_op jit(solution)/shard_map/all_to_all | solution.py:176
  291.9 2.1 convert_reduce_fusion
  294.1 3.7 %collective-permute-start.10 = (bf16[128,1024]{1,0:T(8,128)(2,1)S(1)}, bf16[128,1024]{1,0:T(8,128)(2,1)S(1)}, u32[]{:S(2)}, u32[]{:S(2)}) collective-permute-start(bf16[128,1024]{1,0:T(8,128)(2,1)S(1)} %slice.104), channel_id=1, source_target_pairs={{0,480},{1,33},{2,482},{3,35},{4,484},{5,37},{6,486},{7,39},{8,488... | collective-permute-start | bytes 786440 | tf_op jit(solution)/shard_map/ppermute | solution.py:115
  298.0 13.4 %collective-permute-start.8 = (bf16[64,1024]{1,0:T(8,128)(2,1)S(1)}, bf16[64,1024]{1,0:T(8,128)(2,1)S(1)}, u32[]{:S(2)}, u32[]{:S(2)}) collective-permute-start(bf16[64,1024]{1,0:T(8,128)(2,1)S(1)} %slice.107), channel_id=1, source_target_pairs={{0,448},{1,65},{2,450},{3,67},{4,452},{5,69},{6,454},{7,71},{8,456... | collective-permute-start | bytes 393224 | tf_op jit(solution)/shard_map/ppermute | solution.py:115
  311.6 3.2 collective-permute-start.11
  314.8 5.4 %collective-permute-start.9 = (bf16[32,1024]{1,0:T(8,128)(2,1)S(1)}, bf16[32,1024]{1,0:T(8,128)(2,1)S(1)}, u32[]{:S(2)}, u32[]{:S(2)}) collective-permute-start(bf16[32,1024]{1,0:T(8,128)(2,1)S(1)} %slice.109), channel_id=1, source_target_pairs={{0,384},{1,129},{2,386},{3,131},{4,388},{5,133},{6,390},{7,135},{8... | collective-permute-start | bytes 196616 | tf_op jit(solution)/shard_map/ppermute | solution.py:115
  320.3 7.0 %collective-permute-start.12 = (bf16[32,1024]{1,0:T(8,128)(2,1)S(1)}, bf16[32,1024]{1,0:T(8,128)(2,1)S(1)}, u32[]{:S(2)}, u32[]{:S(2)}) collective-permute-start(bf16[32,1024]{1,0:T(8,128)(2,1)S(1)} %slice.108), channel_id=1, source_target_pairs={{0,384},{1,129},{2,386},{3,131},{4,388},{5,133},{6,390},{7,135},{8... | collective-permute-start | bytes 196616 | tf_op jit(solution)/shard_map/ppermute | solution.py:115
  327.4 1.8 collective-permute-done.12
  330.2 5.5 %all-to-all-start.6 = ((bf16[8,32,1024]{2,1,0:T(8,128)(2,1)}), bf16[8,32,1024]{2,1,0:T(8,128)(2,1)S(1)}, u32[]{:S(2)}, u32[]{:S(2)}) async-start(bf16[8,32,1024]{2,1,0:T(8,128)(2,1)} %broadcast_in_dim.83), calls=%async_computation.6 | async-start | bytes 1048576 | tf_op jit(solution)/shard_map/all_to_all | solution.py:184
  335.7 1.3 copy.19
  337.0 1.3 copy.20
  338.2 6.9 %all-to-all-done.6 = bf16[8,32,1024]{2,1,0:T(8,128)(2,1)S(1)} async-done(((bf16[8,32,1024]{2,1,0:T(8,128)(2,1)}), bf16[8,32,1024]{2,1,0:T(8,128)(2,1)S(1)}, u32[]{:S(2)}, u32[]{:S(2)}) %all-to-all-start.6) | async-done | bytes 524320 | tf_op jit(solution)/shard_map/all_to_all | solution.py:184
  345.9 4.4 %all-to-all-start.4 = ((bf16[8,32,1024]{2,1,0:T(8,128)(2,1)}), bf16[8,32,1024]{2,1,0:T(8,128)(2,1)S(1)}, u32[]{:S(2)}, u32[]{:S(2)}) async-start(bf16[8,32,1024]{2,1,0:T(8,128)(2,1)} %broadcast_in_dim.82), calls=%async_computation.4 | async-start | bytes 1048576 | tf_op jit(solution)/shard_map/all_to_all | solution.py:184
  351.6 8.1 %all-to-all-done.4 = bf16[8,32,1024]{2,1,0:T(8,128)(2,1)S(1)} async-done(((bf16[8,32,1024]{2,1,0:T(8,128)(2,1)}), bf16[8,32,1024]{2,1,0:T(8,128)(2,1)S(1)}, u32[]{:S(2)}, u32[]{:S(2)}) %all-to-all-start.4) | async-done | bytes 524320 | tf_op jit(solution)/shard_map/all_to_all | solution.py:184
  (70 shorter events, 10.7 us)
Async XLA Ops:
  1.4 1.2 copy-start.2
  2.5 1.2 copy-start.3
  7.5 10.4 %copy-start.9 = (f32[8,224,128]{2,1,0:T(8,128)S(1)}, f32[8,224,128]{2,1,0:T(8,128)}, u32[]{:S(2)}) copy-start(f32[8,224,128]{2,1,0:T(8,128)} %param.13) | copy-start | bytes 2752516
  7.5 24.0 %all-to-all-start = ((bf16[8,4,112,128]{3,2,1,0:T(8,128)(2,1)}), bf16[8,4,112,128]{3,2,1,0:T(8,128)(2,1)S(1)}, u32[]{:S(2)}, u32[]{:S(2)}) async-start(bf16[8,4,112,128]{3,2,1,0:T(8,128)(2,1)} %pack.1), calls=%async_computation | async-start | bytes 1835008 | tf_op jit(solution)/shard_map/all_to_all | solution.py:146
  31.5 13.0 %all-to-all-start.2 = ((bf16[8,224,128]{2,1,0:T(8,128)(2,1)}), bf16[8,224,128]{2,1,0:T(8,128)(2,1)S(1)}, u32[]{:S(2)}, u32[]{:S(2)}) async-start(bf16[8,224,128]{2,1,0:T(8,128)(2,1)} %convert_element_type.76), calls=%async_computation.2 | async-start | bytes 917504 | tf_op jit(solution)/shard_map/all_to_all | solution.py:140
  37.3 21.2 %copy-start.10 = (s32[128,2]{0,1:T(2,128)S(1)}, s32[128,2]{0,1:T(2,128)}, u32[]{:S(2)}) copy-start(s32[128,2]{0,1:T(2,128)} %param.8) | copy-start | bytes 3076
  37.3 21.5 %copy-start.8 = (bf16[128,2048]{1,0:T(8,128)(2,1)S(1)}, bf16[128,2048]{1,0:T(8,128)(2,1)}, u32[]{:S(2)}) copy-start(bf16[128,2048]{1,0:T(8,128)(2,1)} %param.7) | copy-start | bytes 1572868
  44.5 180.0 %all-to-all-start.1 = ((bf16[64,112,128]{2,1,0:T(8,128)(2,1)}), bf16[64,112,128]{2,1,0:T(8,128)(2,1)S(1)}, u32[]{:S(2)}, u32[]{:S(2)}) async-start(bf16[64,112,128]{2,1,0:T(8,128)(2,1)} %pad_maximum_fusion), calls=%async_computation.1 | async-start | bytes 3670016 | tf_op jit(solution)/shard_map/all_to_all | solution.py:148
  59.3 88.2 %collective-permute-start = (bf16[32,2048]{1,0:T(8,128)(2,1)S(1)}, bf16[32,2048]{1,0:T(8,128)(2,1)S(1)}, u32[]{:S(2)}, u32[]{:S(2)}) collective-permute-start(bf16[32,2048]{1,0:T(8,128)(2,1)S(1)} %convolution_convert_fusion), channel_id=1, source_target_pairs={{0,128},{1,385},{2,130},{3,387},{4,132},{5,389},{6,134},{7,391},{8... | collective-permute-start | bytes 393224 | tf_op jit(solution)/shard_map/ppermute | solution.py:115
  147.5 9.3 %collective-permute-start.1 = (bf16[64,2048]{1,0:T(8,128)(2,1)S(1)}, bf16[64,2048]{1,0:T(8,128)(2,1)S(1)}, u32[]{:S(2)}, u32[]{:S(2)}) collective-permute-start(bf16[64,2048]{1,0:T(8,128)(2,1)S(1)} %pad_maximum_fusion.4), channel_id=1, source_target_pairs={{0,64},{1,449},{2,66},{3,451},{4,68},{5,453},{6,70},{7,455},{8,72}... | collective-permute-start | bytes 786440 | tf_op jit(solution)/shard_map/ppermute | solution.py:115
  156.9 11.3 %collective-permute-start.2 = (bf16[128,2048]{1,0:T(8,128)(2,1)S(1)}, bf16[128,2048]{1,0:T(8,128)(2,1)S(1)}, u32[]{:S(2)}, u32[]{:S(2)}) collective-permute-start(bf16[128,2048]{1,0:T(8,128)(2,1)S(1)} %pad_maximum_fusion.2), channel_id=1, source_target_pairs={{0,32},{1,481},{2,34},{3,483},{4,36},{5,485},{6,38},{7,487},{8,40}... | collective-permute-start | bytes 1572872 | tf_op jit(solution)/shard_map/ppermute | solution.py:115
  169.2 24.3 %collective-permute-start.3 = (bf16[256,2048]{1,0:T(8,128)(2,1)}, bf16[256,2048]{1,0:T(8,128)(2,1)}, u32[]{:S(2)}, u32[]{:S(2)}) collective-permute-start(bf16[256,2048]{1,0:T(8,128)(2,1)} %pad_maximum_fusion.1), channel_id=1, source_target_pairs={{0,8},{1,9},{2,10},{3,11},{4,12},{5,13},{6,14},{7,15},{8,16},{9,17... | collective-permute-start | bytes 3145736 | tf_op jit(solution)/shard_map/ppermute | solution.py:118
  172.2 45.1 %collective-permute-start.4 = (bf16[256,2048]{1,0:T(8,128)(2,1)}, bf16[256,2048]{1,0:T(8,128)(2,1)}, u32[]{:S(2)}, u32[]{:S(2)}) collective-permute-start(bf16[256,2048]{1,0:T(8,128)(2,1)} %pad_maximum_fusion.1), channel_id=1, source_target_pairs={{0,16},{1,17},{2,18},{3,19},{4,20},{5,21},{6,22},{7,23},{8,24},{9,... | collective-permute-start | bytes 3145736 | tf_op jit(solution)/shard_map/ppermute | solution.py:118
  177.7 46.8 %collective-permute-start.6 = (bf16[224,1024]{1,0:T(8,128)(2,1)S(1)}, bf16[224,1024]{1,0:T(8,128)(2,1)}, u32[]{:S(2)}, u32[]{:S(2)}) collective-permute-start(bf16[224,1024]{1,0:T(8,128)(2,1)S(1)} %copy_bitcast_fusion), channel_id=1, source_target_pairs={{0,256},{1,257},{2,258},{3,259},{4,260},{5,261},{6,262},{7,263},{8... | collective-permute-start | bytes 1376264 | tf_op jit(solution)/shard_map/ppermute | solution.py:143
  185.7 36.7 %collective-permute-start.5 = (bf16[256,2048]{1,0:T(8,128)(2,1)}, bf16[256,2048]{1,0:T(8,128)(2,1)S(1)}, u32[]{:S(2)}, u32[]{:S(2)}) collective-permute-start(bf16[256,2048]{1,0:T(8,128)(2,1)} %pad_maximum_fusion.1), channel_id=1, source_target_pairs={{0,24},{1,25},{2,26},{3,27},{4,28},{5,29},{6,30},{7,31},{8,0},{9,1... | collective-permute-start | bytes 3145736 | tf_op jit(solution)/shard_map/ppermute | solution.py:118
  222.5 2.0 copy-start.4
  225.1 4.1 %copy-start = (bf16[1,2048,224]{2,1,0:T(8,128)(2,1)}, bf16[1,2048,224]{2,1,0:T(8,128)(2,1)S(1)}, u32[]{:S(2)}) copy-start(bf16[1,2048,224]{2,1,0:T(8,128)(2,1)S(1)} %get-tuple-element.24) | copy-start | bytes 2752516
  225.1 4.1 %copy-start.5 = (bf16[4,256,2048]{2,1,0:T(8,128)(2,1)S(1)}, bf16[4,256,2048]{2,1,0:T(8,128)(2,1)}, u32[]{:S(2)}) copy-start(bf16[4,256,2048]{2,1,0:T(8,128)(2,1)} %copy-done.4) | copy-start | bytes 12582916
  232.0 6.7 %copy-start.6 = (bf16[224,1024]{1,0:T(8,128)(2,1)}, bf16[224,1024]{1,0:T(8,128)(2,1)S(1)}, u32[]{:S(2)}) copy-start(bf16[224,1024]{1,0:T(8,128)(2,1)S(1)} %get-tuple-element.29) | copy-start | bytes 1376260
  234.1 29.4 %all-to-all-start.3 = ((bf16[4,256,1024]{2,1,0:T(8,128)(2,1)}), bf16[4,256,1024]{2,1,0:T(8,128)(2,1)}, u32[]{:S(2)}, u32[]{:S(2)}) async-start(bf16[4,256,1024]{2,1,0:T(8,128)(2,1)} %bitcast.58), calls=%async_computation.3 | async-start | bytes 4194304 | tf_op jit(solution)/shard_map/all_to_all | solution.py:176
  263.5 4.6 %copy-start.11 = (f32[128,2]{0,1:T(2,128)S(1)}, f32[128,2]{0,1:T(2,128)}, u32[]{:S(2)}) copy-start(f32[128,2]{0,1:T(2,128)} %param.9) | copy-start | bytes 3076
  263.5 28.4 %all-to-all-start.5 = ((bf16[4,256,1024]{2,1,0:T(8,128)(2,1)}), bf16[4,256,1024]{2,1,0:T(8,128)(2,1)}, u32[]{:S(2)}, u32[]{:S(2)}) async-start(bf16[4,256,1024]{2,1,0:T(8,128)(2,1)} %bitcast.57), calls=%async_computation.5 | async-start | bytes 4194304 | tf_op jit(solution)/shard_map/all_to_all | solution.py:176
  270.3 27.6 %collective-permute-start.7 = (bf16[128,1024]{1,0:T(8,128)(2,1)S(1)}, bf16[128,1024]{1,0:T(8,128)(2,1)S(1)}, u32[]{:S(2)}, u32[]{:S(2)}) collective-permute-start(bf16[128,1024]{1,0:T(8,128)(2,1)S(1)} %slice.105), channel_id=1, source_target_pairs={{0,480},{1,33},{2,482},{3,35},{4,484},{5,37},{6,486},{7,39},{8,488... | collective-permute-start | bytes 786440 | tf_op jit(solution)/shard_map/ppermute | solution.py:115
  294.1 17.4 %collective-permute-start.10 = (bf16[128,1024]{1,0:T(8,128)(2,1)S(1)}, bf16[128,1024]{1,0:T(8,128)(2,1)S(1)}, u32[]{:S(2)}, u32[]{:S(2)}) collective-permute-start(bf16[128,1024]{1,0:T(8,128)(2,1)S(1)} %slice.104), channel_id=1, source_target_pairs={{0,480},{1,33},{2,482},{3,35},{4,484},{5,37},{6,486},{7,39},{8,488... | collective-permute-start | bytes 786440 | tf_op jit(solution)/shard_map/ppermute | solution.py:115
  298.0 16.8 %collective-permute-start.8 = (bf16[64,1024]{1,0:T(8,128)(2,1)S(1)}, bf16[64,1024]{1,0:T(8,128)(2,1)S(1)}, u32[]{:S(2)}, u32[]{:S(2)}) collective-permute-start(bf16[64,1024]{1,0:T(8,128)(2,1)S(1)} %slice.107), channel_id=1, source_target_pairs={{0,448},{1,65},{2,450},{3,67},{4,452},{5,69},{6,454},{7,71},{8,456... | collective-permute-start | bytes 393224 | tf_op jit(solution)/shard_map/ppermute | solution.py:115
  311.5 24.2 %copy-start.1 = (bf16[1,2048,224]{2,1,0:T(8,128)(2,1)S(1)}, bf16[1,2048,224]{2,1,0:T(8,128)(2,1)}, u32[]{:S(2)}) copy-start(bf16[1,2048,224]{2,1,0:T(8,128)(2,1)} %copy-done) | copy-start | bytes 2752516
  311.6 8.7 %collective-permute-start.11 = (bf16[64,1024]{1,0:T(8,128)(2,1)S(1)}, bf16[64,1024]{1,0:T(8,128)(2,1)S(1)}, u32[]{:S(2)}, u32[]{:S(2)}) collective-permute-start(bf16[64,1024]{1,0:T(8,128)(2,1)S(1)} %slice.106), channel_id=1, source_target_pairs={{0,448},{1,65},{2,450},{3,67},{4,452},{5,69},{6,454},{7,71},{8,456... | collective-permute-start | bytes 393224 | tf_op jit(solution)/shard_map/ppermute | solution.py:115
  314.8 12.5 %collective-permute-start.9 = (bf16[32,1024]{1,0:T(8,128)(2,1)S(1)}, bf16[32,1024]{1,0:T(8,128)(2,1)S(1)}, u32[]{:S(2)}, u32[]{:S(2)}) collective-permute-start(bf16[32,1024]{1,0:T(8,128)(2,1)S(1)} %slice.109), channel_id=1, source_target_pairs={{0,384},{1,129},{2,386},{3,131},{4,388},{5,133},{6,390},{7,135},{8... | collective-permute-start | bytes 196616 | tf_op jit(solution)/shard_map/ppermute | solution.py:115
  320.3 9.0 %collective-permute-start.12 = (bf16[32,1024]{1,0:T(8,128)(2,1)S(1)}, bf16[32,1024]{1,0:T(8,128)(2,1)S(1)}, u32[]{:S(2)}, u32[]{:S(2)}) collective-permute-start(bf16[32,1024]{1,0:T(8,128)(2,1)S(1)} %slice.108), channel_id=1, source_target_pairs={{0,384},{1,129},{2,386},{3,131},{4,388},{5,133},{6,390},{7,135},{8... | collective-permute-start | bytes 196616 | tf_op jit(solution)/shard_map/ppermute | solution.py:115
  330.2 14.9 %all-to-all-start.6 = ((bf16[8,32,1024]{2,1,0:T(8,128)(2,1)}), bf16[8,32,1024]{2,1,0:T(8,128)(2,1)S(1)}, u32[]{:S(2)}, u32[]{:S(2)}) async-start(bf16[8,32,1024]{2,1,0:T(8,128)(2,1)} %broadcast_in_dim.83), calls=%async_computation.6 | async-start | bytes 1048576 | tf_op jit(solution)/shard_map/all_to_all | solution.py:184
  336.9 13.3 %copy-start.7 = (bf16[224,1024]{1,0:T(8,128)(2,1)S(1)}, bf16[224,1024]{1,0:T(8,128)(2,1)}, u32[]{:S(2)}) copy-start(bf16[224,1024]{1,0:T(8,128)(2,1)} %copy-done.6) | copy-start | bytes 1376260
  345.9 13.7 %all-to-all-start.4 = ((bf16[8,32,1024]{2,1,0:T(8,128)(2,1)}), bf16[8,32,1024]{2,1,0:T(8,128)(2,1)S(1)}, u32[]{:S(2)}, u32[]{:S(2)}) async-start(bf16[8,32,1024]{2,1,0:T(8,128)(2,1)} %broadcast_in_dim.82), calls=%async_computation.4 | async-start | bytes 1048576 | tf_op jit(solution)/shard_map/all_to_all | solution.py:184
where the time goes:
time: 365 us; the launch traced here: 361 us
  waiting for transfers between devices  204 us (56%)
  starting transfers between devices  116 us (32%)
  local copies, waits for them, and re-layouts  12.8 us (4%)
  other arithmetic  11.7 us (3%)
  matrix products  10.7 us (3%)
  Pallas kernels  4.32 us (1%)
    ppermute x9, waiting for transfers between devices, along_z(): return lax.ppermute(x, ALL, pairs)  97.5 us
    ppermute x9, starting transfers between devices, along_z(): return lax.ppermute(x, ALL, pairs)  50.1 us
    all_to_all x2, waiting for transfers between devices, local(): lax.all_to_all(sums.reshape(fs_1, -1, sums.shape[1]), 'fs_1', 0, 0, tiled...  40.2 us
    ppermute x3, waiting for transfers between devices, along_y(): lax.ppermute(x, ALL, permutation(sizes, lambda z, y, t: (z, y + hops)))  31.4 us
    all_to_all x2, waiting for transfers between devices, local(): lax.all_to_all(jnp.broadcast_to(block[None], (tp_size, *block.shape)), 't...  15 us
    all_to_all x1, starting transfers between devices, local(): tiles = lax.all_to_all(tiles, GR_FS, 0, 0, tiled=True)  13.9 us
    all_to_all x1, waiting for transfers between devices, local(): lax.all_to_all(tiles, 'tp', 0, 0, tiled=True).reshape(-1, 112, LANES)  12.8 us
    all_to_all x1, starting transfers between devices, local(): lax.all_to_all(tiles, 'tp', 0, 0, tiled=True).reshape(-1, 112, LANES)  10.4 us
  transfers between devices with their start and end apart: 20, of which 13 were waited for; matrix products, arithmetic and copies ran while one was open for 5% of the time, Pallas kernels for 0%

commit v1 on v0

--- a/solution.py
+++ b/solution.py
@@ -37,8 +37,8 @@
         tail = lane_window(blocks, 224 * j + LANES)
         last = tail[48:]
         spread = jnp.concatenate([pltpu.roll(last, 96 - 32 * q, 1) for q in range(3)], axis=0)
-        out_ref[0, j, :64, :] = main.astype(jnp.bfloat16)
-        out_ref[0, j, 64:, :] = jnp.where(lane < 96, tail[:48], spread).astype(jnp.bfloat16)
+        out_ref[0, 112 * j : 112 * j + 64, :] = main.astype(jnp.bfloat16)
+        out_ref[0, 112 * j + 64 : 112 * j + 112, :] = jnp.where(lane < 96, tail[:48], spread).astype(jnp.bfloat16)
 
 
 def pack(gate_master, up_master, gain):
@@ -51,8 +51,8 @@
             pl.BlockSpec((1, rows, cols), lambda i: (i, 0, 0)),
             pl.BlockSpec((rows, 1), lambda i: (0, 0)),
         ],
-        out_specs=pl.BlockSpec((1, 4, 112, LANES), lambda i: (i, 0, 0, 0)),
-        out_shape=jax.ShapeDtypeStruct((experts, 4, 112, LANES), jnp.bfloat16),
+        out_specs=pl.BlockSpec((1, 448, LANES), lambda i: (i, 0, 0)),
+        out_shape=jax.ShapeDtypeStruct((experts, 448, LANES), jnp.bfloat16),
         cost_estimate=pl.CostEstimate(flops=4000000, bytes_accessed=2800000, transcendentals=0),
         compiler_params=pltpu.CompilerParams(vmem_limit_bytes=4 * 2**20),
         name="pack",
@@ -132,12 +132,11 @@
     weight_rows = jnp.sum(jnp.where(route_hits, route_weight[None, :, :], 0.0), axis=2)
     mine = lax.axis_index("tp")
     my_picker = lax.dynamic_index_in_dim(picker, mine, 0, keepdims=False)
-    my_weights = lax.dynamic_index_in_dim(weight_rows, mine, 0, keepdims=False)
-    slot_weight = jnp.sum(jnp.where(my_picker, my_weights[None, :], 0.0), axis=1)
+    slot_weight = jnp.sum(jnp.where(picker, weight_rows[:, None, :], 0.0), axis=2)
     packed = jnp.dot(my_picker.astype(bf16), normed, preferred_element_type=f32).astype(bf16)
 
-    down_half = down_master.astype(bf16)
-    down_tiles = lax.all_to_all(down_half, "tp", 0, 0, tiled=True)
+    down_tiles = down_master.astype(bf16)
+    down_tiles = lax.all_to_all(down_tiles, "tp", 0, 0, tiled=True)
     down_own = jnp.moveaxis(down_tiles, 0, 1).reshape(down_tiles.shape[1], -1)
     across = permutation(sizes, lambda z, y, t: (z + sizes[1], y))
     down_other = lax.ppermute(down_own, ALL, across)
@@ -159,40 +158,59 @@
             moved = along_y(held, k)
         gathered = lax.dynamic_update_index_in_dim(gathered, moved, (row + fs_1 - k) % fs_1, 0)
     gathered = gathered.reshape(-1, gathered.shape[2])
-    tiles, gathered, down_other = lax.optimization_barrier((tiles, gathered, down_other))
-
+    low = lax.axis_index("gr") == 0
+    down_weight = jnp.concatenate(
+        [jnp.where(low, down_own, down_other), jnp.where(low, down_other, down_own)], axis=1
+    )
+    columns = down_weight.shape[1] // fs_1
+    down_cols = []
+    for k in range(fs_1):
+        picked = lax.dynamic_slice_in_dim(down_weight, (row + k) % fs_1 * columns, columns, axis=1)
+        if k:
+            picked = along_y(picked, k)
+        down_cols.append(picked)
+    tiles, gathered = lax.optimization_barrier((tiles, gathered))
     gate_weight, up_weight = unpack(tiles)
-    low = lax.axis_index("gr") == 0
-    down_parts = [jnp.where(low, down_own, down_other), jnp.where(low, down_other, down_own)]
-    down_weight = jnp.concatenate(down_parts, axis=1)[None]
 
     gate_act = jnp.dot(gathered, gate_weight[0], preferred_element_type=f32)
     up_act = jnp.dot(gathered, up_weight[0], preferred_element_type=f32)
     hidden = (jax.nn.silu(gate_act) * up_act).astype(bf16)
-    everyone = picker.reshape(-1, picker.shape[2]).astype(bf16)
-    mixed = []
-    for part in down_parts:
-        sums = jnp.dot(hidden, part, preferred_element_type=f32).astype(bf16)
-        sums = lax.all_to_all(sums.reshape(fs_1, -1, sums.shape[1]), "fs_1", 0, 0, tiled=True)
-        total = jnp.sum(sums.astype(f32), axis=0)
-        for hops in (1, 2, 4):
-            half = total.shape[0] // 2
-            moved = along_z(total[half:].astype(bf16), -hops)
-            total = total[:half] + moved.astype(f32)
-        block = (total * slot_weight[:, None]).astype(bf16)
-        block, slot_weight = lax.optimization_barrier((block, slot_weight))
-        blocks = lax.all_to_all(
-            jnp.broadcast_to(block[None], (tp_size, *block.shape)), "tp", 0, 0, tiled=True
-        )
-        mixed.append(
-            lax.dot_general(
-                everyone,
-                blocks.reshape(-1, blocks.shape[2]),
-                (((0,), (0,)), ((), ())),
-                preferred_element_type=f32,
-            ).astype(bf16)
-        )
-    return (gate_weight, up_weight, down_weight, jnp.concatenate(mixed, axis=1))
+    hidden = hidden.reshape(fs_1, -1, hidden.shape[1])
+    half = hidden.shape[1] // 2
+
+    def over_hidden(part):
+        total = 0.0
+        for k in range(fs_1):
+            moved = part
+            if k:
+                moved = along_y(part, k)
+            total = total + jnp.dot(
+                moved.reshape(-1, moved.shape[2]), down_cols[k], preferred_element_type=f32
+            )
+        return total.reshape(fs_1, -1, columns)
+
+    odd = over_hidden(hidden[:, half:])
+    total = over_hidden(hidden[:, :half])
+    for hops in (1, 2, 4):
+        moved = along_z(odd.astype(bf16), -hops)
+        total = total + moved.astype(f32)
+        half = total.shape[1] // 2
+        total, odd = total[:, :half], total[:, half:]
+        if hops == 4:
+            total = jnp.concatenate([total, odd], axis=1)
+
+    block = total.astype(bf16)
+    block = jnp.broadcast_to(block[:, None], (fs_1, tp_size, *block.shape[1:]))
+    blocks = lax.all_to_all(block.reshape(-1, *block.shape[2:]), ("fs_1", "tp"), 0, 0, tiled=True)
+    blocks = blocks.reshape(fs_1, -1, columns).astype(f32) * slot_weight.reshape(1, -1, 1)
+    blocks = jnp.moveaxis(blocks.astype(bf16), 0, 1).reshape(-1, fs_1 * columns)
+    mixed = lax.dot_general(
+        picker.reshape(-1, picker.shape[2]).astype(bf16),
+        blocks,
+        (((0,), (0,)), ((), ())),
+        preferred_element_type=f32,
+    ).astype(bf16)
+    return (gate_weight, up_weight, down_weight[None], mixed)
 
 
 def solution(mesh):

time: 365 us -> 362 us (level)
  starting transfers between devices: 116 us -> 111 us
  matrix products: 10.7 us -> 15.1 us
    all_to_all x5 -> x2, waiting for transfers between devices: 62.4 us -> 20.6 us  [the longest x1 13.3 us: local(): lax.all_to_all(block.reshape(-1, *block.shape[2:]), ('fs_1', 'tp'), 0, 0,...]
    ppermute x3 -> x12, starting transfers between devices: 10.3 us -> 42.3 us  [along_y(): lax.ppermute(x, ALL, permutation(sizes, lambda z, y, t: (z, y + hops)))]
    ppermute x1, waiting for transfers between devices: 0.01 us -> 30.8 us  [local(): down_other = lax.ppermute(down_own, ALL, across)]
    ppermute x9 -> x6, starting transfers between devices: 50.1 us -> 19.3 us  [along_z(): return lax.ppermute(x, ALL, pairs)]
    ppermute x9 -> x6, waiting for transfers between devices: 97.5 us -> 115 us  [along_z(): return lax.ppermute(x, ALL, pairs)]
    ppermute x3 -> x12, waiting for transfers between devices: 31.4 us -> 22.8 us  [along_y(): lax.ppermute(x, ALL, permutation(sizes, lambda z, y, t: (z, y + hops)))]
    all_to_all x5 -> x2, starting transfers between devices: 23.3 us -> 16.8 us  [the longest x1 12.5 us: local(): lax.all_to_all(block.reshape(-1, *block.shape[2:]), ('fs_1', 'tp'), 0, 0,...]
    reduce_sum x3 -> x1, other arithmetic: 4.31 us -> 0.11 us  [local(): jnp.sum(jnp.where(picker, weight_rows[:, None, :], 0.0), axis=2)]
  transfers between devices with their start and end apart: 20 -> 23, of which waited for: 13 -> 11; matrix products, arithmetic and copies ran while one was open for 5% -> 9% of each run, Pallas kernels for 0% -> 0%
where the time goes in v1:
time: 362 us; the launch traced here: 360 us
  waiting for transfers between devices  202 us (56%)
  starting transfers between devices  111 us (31%)
  local copies, waits for them, and re-layouts  16.2 us (4%)
  matrix products  15.1 us (4%)
  other arithmetic  10.2 us (3%)
  Pallas kernels  4.32 us (1%)
    ppermute x6, waiting for transfers between devices, along_z(): return lax.ppermute(x, ALL, pairs)  115 us
    ppermute x12, starting transfers between devices, along_y(): lax.ppermute(x, ALL, permutation(sizes, lambda z, y, t: (z, y + hops)))  42.3 us
    ppermute x1, waiting for transfers between devices, local(): down_other = lax.ppermute(down_own, ALL, across)  30.8 us
    ppermute x12, waiting for transfers between devices, along_y(): lax.ppermute(x, ALL, permutation(sizes, lambda z, y, t: (z, y + hops)))  22.8 us
    ppermute x6, starting transfers between devices, along_z(): return lax.ppermute(x, ALL, pairs)  19.3 us
    all_to_all x1, starting transfers between devices, local(): tiles = lax.all_to_all(tiles, GR_FS, 0, 0, tiled=True)  13.9 us
    all_to_all x1, waiting for transfers between devices, local(): lax.all_to_all(block.reshape(-1, *block.shape[2:]), ('fs_1', 'tp'), 0, 0,...  13.3 us
    all_to_all x1, waiting for transfers between devices, local(): lax.all_to_all(tiles, 'tp', 0, 0, tiled=True).reshape(-1, 112, LANES)  12.8 us
  transfers between devices with their start and end apart: 23, of which 11 were waited for; matrix products, arithmetic and copies ran while one was open for 9% of the time, Pallas kernels for 0%

profile of v1, /device:TPU:1, one launch (start us, length us, event | category | flops | bytes accessed | tf_op | source)
XLA Modules:
  0.0 360.1 jit_solution(9943052267825561720)
XLA Ops:
  3.7 3.7 %pack.1 = bf16[8,448,128]{2,1,0:T(8,128)(2,1)} custom-call(f32[8,32,896]{2,1,0:T(8,128)S(1)} %copy-done.2, f32[8,32,896]{2,1,0:T(8,128)S(1)} %copy-done.3, f32[32,1]{1,0:T(8,128)S(1)} %copy.30.gain_ref), custom_call_target="tpu_custom_call" | custom-call | flops 4000000 | bytes 2800000 | tf_op jit(solution)/shard_map/pack/pallas_call | solution.py:46
  7.5 10.3 %all-to-all-start = ((bf16[8,448,128]{2,1,0:T(8,128)(2,1)}), bf16[8,448,128]{2,1,0:T(8,128)(2,1)S(1)}, u32[]{:S(2)}, u32[]{:S(2)}) async-start(bf16[8,448,128]{2,1,0:T(8,128)(2,1)} %pack.1), calls=%async_computation | async-start | bytes 1835008 | tf_op jit(solution)/shard_map/all_to_all | solution.py:145
  18.6 12.8 %all-to-all-done = bf16[8,448,128]{2,1,0:T(8,128)(2,1)S(1)} async-done(((bf16[8,448,128]{2,1,0:T(8,128)(2,1)}), bf16[8,448,128]{2,1,0:T(8,128)(2,1)S(1)}, u32[]{:S(2)}, u32[]{:S(2)}) %all-to-all-start) | async-done | bytes 917536 | tf_op jit(solution)/shard_map/all_to_all | solution.py:145
  31.4 4.3 %all-to-all-start.2 = ((bf16[8,224,128]{2,1,0:T(8,128)(2,1)}), bf16[8,224,128]{2,1,0:T(8,128)(2,1)S(1)}, u32[]{:S(2)}, u32[]{:S(2)}) async-start(bf16[8,224,128]{2,1,0:T(8,128)(2,1)} %convert_element_type.60), calls=%async_computation.2 | async-start | bytes 917504 | tf_op jit(solution)/shard_map/all_to_all | solution.py:139
  35.7 1.4 pad_maximum_fusion
  37.1 7.3 %all-to-all-done.2 = bf16[8,224,128]{2,1,0:T(8,128)(2,1)S(1)} async-done(((bf16[8,224,128]{2,1,0:T(8,128)(2,1)}), bf16[8,224,128]{2,1,0:T(8,128)(2,1)S(1)}, u32[]{:S(2)}, u32[]{:S(2)}) %all-to-all-start.2) | async-done | bytes 458784 | tf_op jit(solution)/shard_map/all_to_all | solution.py:139
  44.4 13.9 %all-to-all-start.1 = ((bf16[64,112,128]{2,1,0:T(8,128)(2,1)}), bf16[64,112,128]{2,1,0:T(8,128)(2,1)S(1)}, u32[]{:S(2)}, u32[]{:S(2)}) async-start(bf16[64,112,128]{2,1,0:T(8,128)(2,1)} %pad_maximum_fusion), calls=%async_computation.1 | async-start | bytes 3670016 | tf_op jit(solution)/shard_map/all_to_all | solution.py:147
  59.2 7.0 %collective-permute-start = (bf16[32,2048]{1,0:T(8,128)(2,1)S(1)}, bf16[32,2048]{1,0:T(8,128)(2,1)S(1)}, u32[]{:S(2)}, u32[]{:S(2)}) collective-permute-start(bf16[32,2048]{1,0:T(8,128)(2,1)S(1)} %convolution_convert_fusion.1), channel_id=1, source_target_pairs={{0,128},{1,385},{2,130},{3,387},{4,132},{5,389},{6,134},{7,391},{8... | collective-permute-start | bytes 393224 | tf_op jit(solution)/shard_map/ppermute | solution.py:115
  66.2 81.2 %collective-permute-done = bf16[32,2048]{1,0:T(8,128)(2,1)S(1)} collective-permute-done((bf16[32,2048]{1,0:T(8,128)(2,1)S(1)}, bf16[32,2048]{1,0:T(8,128)(2,1)S(1)}, u32[]{:S(2)}, u32[]{:S(2)}) %collective-permute-start) | collective-permute-done | bytes 131104 | tf_op jit(solution)/shard_map/ppermute | solution.py:115
  147.4 1.9 collective-permute-start.1
  149.3 7.4 %collective-permute-done.1 = bf16[64,2048]{1,0:T(8,128)(2,1)S(1)} collective-permute-done((bf16[64,2048]{1,0:T(8,128)(2,1)S(1)}, bf16[64,2048]{1,0:T(8,128)(2,1)S(1)}, u32[]{:S(2)}, u32[]{:S(2)}) %collective-permute-start.1) | collective-permute-done | bytes 262176 | tf_op jit(solution)/shard_map/ppermute | solution.py:115
  156.7 4.2 %collective-permute-start.2 = (bf16[128,2048]{1,0:T(8,128)(2,1)S(1)}, bf16[128,2048]{1,0:T(8,128)(2,1)S(1)}, u32[]{:S(2)}, u32[]{:S(2)}) collective-permute-start(bf16[128,2048]{1,0:T(8,128)(2,1)S(1)} %pad_maximum_fusion.3), channel_id=1, source_target_pairs={{0,32},{1,481},{2,34},{3,483},{4,36},{5,485},{6,38},{7,487},{8,40}... | collective-permute-start | bytes 1572872 | tf_op jit(solution)/shard_map/ppermute | solution.py:115
  161.0 8.7 %collective-permute-start.6 = (bf16[224,1024]{1,0:T(8,128)(2,1)S(1)}, bf16[224,1024]{1,0:T(8,128)(2,1)}, u32[]{:S(2)}, u32[]{:S(2)}) collective-permute-start(bf16[224,1024]{1,0:T(8,128)(2,1)S(1)} %copy_bitcast_fusion), channel_id=1, source_target_pairs={{0,256},{1,257},{2,258},{3,259},{4,260},{5,261},{6,262},{7,263},{8... | collective-permute-start | bytes 1376264 | tf_op jit(solution)/shard_map/ppermute | solution.py:142
  171.7 2.5 collective-permute-start.3
  174.3 5.0 %collective-permute-start.4 = (bf16[256,2048]{1,0:T(8,128)(2,1)}, bf16[256,2048]{1,0:T(8,128)(2,1)S(1)}, u32[]{:S(2)}, u32[]{:S(2)}) collective-permute-start(bf16[256,2048]{1,0:T(8,128)(2,1)} %pad_maximum_fusion.2), channel_id=1, source_target_pairs={{0,16},{1,17},{2,18},{3,19},{4,20},{5,21},{6,22},{7,23},{8,24},{9,... | collective-permute-start | bytes 3145736 | tf_op jit(solution)/shard_map/ppermute | solution.py:118
  179.2 30.8 %collective-permute-done.6 = bf16[224,1024]{1,0:T(8,128)(2,1)} collective-permute-done((bf16[224,1024]{1,0:T(8,128)(2,1)S(1)}, bf16[224,1024]{1,0:T(8,128)(2,1)}, u32[]{:S(2)}, u32[]{:S(2)}) %collective-permute-start.6) | collective-permute-done | bytes 458784 | tf_op jit(solution)/shard_map/ppermute | solution.py:142
  210.0 1.2 broadcast_select_fusion.1
  212.4 2.0 collective-permute-start.8
  214.5 6.4 %collective-permute-start.5 = (bf16[256,2048]{1,0:T(8,128)(2,1)}, bf16[256,2048]{1,0:T(8,128)(2,1)S(1)}, u32[]{:S(2)}, u32[]{:S(2)}) collective-permute-start(bf16[256,2048]{1,0:T(8,128)(2,1)} %pad_maximum_fusion.2), channel_id=1, source_target_pairs={{0,24},{1,25},{2,26},{3,27},{4,28},{5,29},{6,30},{7,31},{8,0},{9,1... | collective-permute-start | bytes 3145736 | tf_op jit(solution)/shard_map/ppermute | solution.py:118
  220.9 2.5 broadcast_in_dim.61
  224.4 2.3 bitcast_dynamic-update-slice_fusion.2
  227.8 20.1 %collective-permute-done.5 = bf16[256,2048]{1,0:T(8,128)(2,1)S(1)} collective-permute-done((bf16[256,2048]{1,0:T(8,128)(2,1)}, bf16[256,2048]{1,0:T(8,128)(2,1)S(1)}, u32[]{:S(2)}, u32[]{:S(2)}) %collective-permute-start.5) | collective-permute-done | bytes 1048608 | tf_op jit(solution)/shard_map/ppermute | solution.py:118
  249.5 4.1 %fusion.11 = f32[1024,224]{0,1:T(8,128)S(1)} fusion(bf16[1024,2048]{1,0:T(8,128)(2,1)} %bitcast.7, bf16[1,2048,224]{2,1,0:T(8,128)(2,1)S(1)} %get-tuple-element.24), kind=kOutput, calls=%fused_computation.30 | convolution fusion | flops 939524096 | bytes 6029312 | tf_op jit(solution)/shard_map/dot_general | solution.py:175
  253.6 3.7 %fusion.6 = bf16[1024,224]{0,1:T(8,128)(2,1)S(1)} fusion(bf16[1024,2048]{1,0:T(8,128)(2,1)} %bitcast.7, bf16[1,2048,224]{2,1,0:T(8,128)(2,1)S(1)} %get-tuple-element.25, f32[1024,224]{0,1:T(8,128)S(1)} %fusion.11), kind=kOutput, calls=%fused_computation.24 | convolution fusion | flops 940900352 | bytes 6488064 | tf_op jit(solution)/shard_map/dot_general | solution.py:176
  258.5 4.5 %collective-permute-start.13 = (bf16[4,128,224]{1,0,2:T(4,128)(2,1)}, bf16[4,128,224]{1,0,2:T(4,128)(2,1)}, u32[]{:S(2)}, u32[]{:S(2)}) collective-permute-start(bf16[4,128,224]{1,0,2:T(4,128)(2,1)} %get-tuple-element.33), channel_id=1, source_target_pairs={{0,8},{1,9},{2,10},{3,11},{4,12},{5,13},{6,14},{7,15},{8,16},{9,17... | collective-permute-start | bytes 688136 | tf_op jit(solution)/shard_map/ppermute | solution.py:118
  263.0 3.8 %collective-permute-start.10 = (bf16[224,512]{1,0:T(8,128)(2,1)}, bf16[224,512]{1,0:T(8,128)(2,1)S(1)}, u32[]{:S(2)}, u32[]{:S(2)}) collective-permute-start(bf16[224,512]{1,0:T(8,128)(2,1)} %get-tuple-element.29), channel_id=1, source_target_pairs={{0,16},{1,17},{2,18},{3,19},{4,20},{5,21},{6,22},{7,23},{8,24},{9,... | collective-permute-start | bytes 688136 | tf_op jit(solution)/shard_map/ppermute | solution.py:118
  266.9 2.4 collective-permute-start.12
  269.3 2.6 collective-permute-start.14
  271.9 4.6 %collective-permute-start.15 = (bf16[4,128,224]{1,0,2:T(4,128)(2,1)}, bf16[4,128,224]{1,0,2:T(4,128)(2,1)S(1)}, u32[]{:S(2)}, u32[]{:S(2)}) collective-permute-start(bf16[4,128,224]{1,0,2:T(4,128)(2,1)} %get-tuple-element.33), channel_id=1, source_target_pairs={{0,24},{1,25},{2,26},{3,27},{4,28},{5,29},{6,30},{7,31},{8,0},{9,1... | collective-permute-start | bytes 688136 | tf_op jit(solution)/shard_map/ppermute | solution.py:118
  276.5 1.9 collective-permute-start.7
  278.4 1.4 fusion.27
  279.9 3.1 collective-permute-start.9
  283.0 3.4 collective-permute-start.11
  287.1 1.3 fusion.5
  288.4 1.9 collective-permute-start.16
  290.4 1.3 fusion.38
  292.0 2.7 collective-permute-done.11
  295.4 4.2 %collective-permute-done.16 = bf16[4,128,512]{2,1,0:T(8,128)(2,1)S(1)} collective-permute-done((bf16[4,128,512]{2,1,0:T(8,128)(2,1)S(1)}, bf16[4,128,512]{2,1,0:T(8,128)(2,1)S(1)}, u32[]{:S(2)}, u32[]{:S(2)}) %collective-permute-start.16) | collective-permute-done | bytes 524320 | tf_op jit(solution)/shard_map/ppermute | solution.py:115
  299.8 1.9 collective-permute-start.17
  301.7 10.1 %collective-permute-done.17 = bf16[4,64,512]{2,1,0:T(8,128)(2,1)S(1)} collective-permute-done((bf16[4,64,512]{2,1,0:T(8,128)(2,1)S(1)}, bf16[4,64,512]{2,1,0:T(8,128)(2,1)S(1)}, u32[]{:S(2)}, u32[]{:S(2)}) %collective-permute-start.17) | collective-permute-done | bytes 262176 | tf_op jit(solution)/shard_map/ppermute | solution.py:115
  311.9 2.3 collective-permute-start.18
  314.2 11.9 %collective-permute-done.18 = bf16[4,32,512]{2,1,0:T(8,128)(2,1)S(1)} collective-permute-done((bf16[4,32,512]{2,1,0:T(8,128)(2,1)S(1)}, bf16[4,32,512]{2,1,0:T(8,128)(2,1)S(1)}, u32[]{:S(2)}, u32[]{:S(2)}) %collective-permute-start.18) | collective-permute-done | bytes 131104 | tf_op jit(solution)/shard_map/ppermute | solution.py:115
  327.3 12.5 %all-to-all-start.3 = ((bf16[32,32,512]{2,1,0:T(8,128)(2,1)}), bf16[32,32,512]{2,1,0:T(8,128)(2,1)}, u32[]{:S(2)}, u32[]{:S(2)}) async-start(bf16[32,32,512]{2,1,0:T(8,128)(2,1)} %bitcast.106), calls=%async_computation.3 | async-start | bytes 2097152 | tf_op jit(solution)/shard_map/all_to_all | solution.py:204
  341.0 1.3 copy.33
  342.3 1.3 copy.34
  343.6 13.3 %all-to-all-done.3 = bf16[32,32,512]{2,1,0:T(8,128)(2,1)} async-done(((bf16[32,32,512]{2,1,0:T(8,128)(2,1)}), bf16[32,32,512]{2,1,0:T(8,128)(2,1)}, u32[]{:S(2)}, u32[]{:S(2)}) %all-to-all-start.3) | async-done | bytes 1048608 | tf_op jit(solution)/shard_map/all_to_all | solution.py:204
  356.9 1.5 fusion.9
  358.9 1.3 convolution_convert_fusion
  (76 shorter events, 17.6 us)
Async XLA Ops:
  1.4 1.2 copy-start.2
  2.5 1.2 copy-start.3
  3.7 14.0 %copy-start.9 = (f32[8,224,128]{2,1,0:T(8,128)S(1)}, f32[8,224,128]{2,1,0:T(8,128)}, u32[]{:S(2)}) copy-start(f32[8,224,128]{2,1,0:T(8,128)} %param.13) | copy-start | bytes 2752516
  7.5 23.9 %all-to-all-start = ((bf16[8,448,128]{2,1,0:T(8,128)(2,1)}), bf16[8,448,128]{2,1,0:T(8,128)(2,1)S(1)}, u32[]{:S(2)}, u32[]{:S(2)}) async-start(bf16[8,448,128]{2,1,0:T(8,128)(2,1)} %pack.1), calls=%async_computation | async-start | bytes 1835008 | tf_op jit(solution)/shard_map/all_to_all | solution.py:145
  31.4 13.0 %all-to-all-start.2 = ((bf16[8,224,128]{2,1,0:T(8,128)(2,1)}), bf16[8,224,128]{2,1,0:T(8,128)(2,1)S(1)}, u32[]{:S(2)}, u32[]{:S(2)}) async-start(bf16[8,224,128]{2,1,0:T(8,128)(2,1)} %convert_element_type.60), calls=%async_computation.2 | async-start | bytes 917504 | tf_op jit(solution)/shard_map/all_to_all | solution.py:139
  37.1 21.2 %copy-start.10 = (s32[128,2]{0,1:T(2,128)S(1)}, s32[128,2]{0,1:T(2,128)}, u32[]{:S(2)}) copy-start(s32[128,2]{0,1:T(2,128)} %param.8) | copy-start | bytes 3076
  37.1 21.5 %copy-start.6 = (bf16[128,2048]{1,0:T(8,128)(2,1)S(1)}, bf16[128,2048]{1,0:T(8,128)(2,1)}, u32[]{:S(2)}) copy-start(bf16[128,2048]{1,0:T(8,128)(2,1)} %param.7) | copy-start | bytes 1572868
  44.4 204.5 %all-to-all-start.1 = ((bf16[64,112,128]{2,1,0:T(8,128)(2,1)}), bf16[64,112,128]{2,1,0:T(8,128)(2,1)S(1)}, u32[]{:S(2)}, u32[]{:S(2)}) async-start(bf16[64,112,128]{2,1,0:T(8,128)(2,1)} %pad_maximum_fusion), calls=%async_computation.1 | async-start | bytes 3670016 | tf_op jit(solution)/shard_map/all_to_all | solution.py:147
  59.2 88.2 %collective-permute-start = (bf16[32,2048]{1,0:T(8,128)(2,1)S(1)}, bf16[32,2048]{1,0:T(8,128)(2,1)S(1)}, u32[]{:S(2)}, u32[]{:S(2)}) collective-permute-start(bf16[32,2048]{1,0:T(8,128)(2,1)S(1)} %convolution_convert_fusion.1), channel_id=1, source_target_pairs={{0,128},{1,385},{2,130},{3,387},{4,132},{5,389},{6,134},{7,391},{8... | collective-permute-start | bytes 393224 | tf_op jit(solution)/shard_map/ppermute | solution.py:115
  147.4 9.3 %collective-permute-start.1 = (bf16[64,2048]{1,0:T(8,128)(2,1)S(1)}, bf16[64,2048]{1,0:T(8,128)(2,1)S(1)}, u32[]{:S(2)}, u32[]{:S(2)}) collective-permute-start(bf16[64,2048]{1,0:T(8,128)(2,1)S(1)} %pad_maximum_fusion.4), channel_id=1, source_target_pairs={{0,64},{1,449},{2,66},{3,451},{4,68},{5,453},{6,70},{7,455},{8,72}... | collective-permute-start | bytes 786440 | tf_op jit(solution)/shard_map/ppermute | solution.py:115
  156.7 13.0 %collective-permute-start.2 = (bf16[128,2048]{1,0:T(8,128)(2,1)S(1)}, bf16[128,2048]{1,0:T(8,128)(2,1)S(1)}, u32[]{:S(2)}, u32[]{:S(2)}) collective-permute-start(bf16[128,2048]{1,0:T(8,128)(2,1)S(1)} %pad_maximum_fusion.3), channel_id=1, source_target_pairs={{0,32},{1,481},{2,34},{3,483},{4,36},{5,485},{6,38},{7,487},{8,40}... | collective-permute-start | bytes 1572872 | tf_op jit(solution)/shard_map/ppermute | solution.py:115
  161.0 49.0 %collective-permute-start.6 = (bf16[224,1024]{1,0:T(8,128)(2,1)S(1)}, bf16[224,1024]{1,0:T(8,128)(2,1)}, u32[]{:S(2)}, u32[]{:S(2)}) collective-permute-start(bf16[224,1024]{1,0:T(8,128)(2,1)S(1)} %copy_bitcast_fusion), channel_id=1, source_target_pairs={{0,256},{1,257},{2,258},{3,259},{4,260},{5,261},{6,262},{7,263},{8... | collective-permute-start | bytes 1376264 | tf_op jit(solution)/shard_map/ppermute | solution.py:142
  169.8 0.8 copy-start.7
  171.7 52.8 %collective-permute-start.3 = (bf16[256,2048]{1,0:T(8,128)(2,1)}, bf16[256,2048]{1,0:T(8,128)(2,1)}, u32[]{:S(2)}, u32[]{:S(2)}) collective-permute-start(bf16[256,2048]{1,0:T(8,128)(2,1)} %pad_maximum_fusion.2), channel_id=1, source_target_pairs={{0,8},{1,9},{2,10},{3,11},{4,12},{5,13},{6,14},{7,15},{8,16},{9,17... | collective-permute-start | bytes 3145736 | tf_op jit(solution)/shard_map/ppermute | solution.py:118
  174.3 52.5 %collective-permute-start.4 = (bf16[256,2048]{1,0:T(8,128)(2,1)}, bf16[256,2048]{1,0:T(8,128)(2,1)S(1)}, u32[]{:S(2)}, u32[]{:S(2)}) collective-permute-start(bf16[256,2048]{1,0:T(8,128)(2,1)} %pad_maximum_fusion.2), channel_id=1, source_target_pairs={{0,16},{1,17},{2,18},{3,19},{4,20},{5,21},{6,22},{7,23},{8,24},{9,... | collective-permute-start | bytes 3145736 | tf_op jit(solution)/shard_map/ppermute | solution.py:118
  211.2 12.1 %copy-start.4 = (bf16[224,1024]{1,0:T(8,128)(2,1)}, bf16[224,1024]{1,0:T(8,128)(2,1)S(1)}, u32[]{:S(2)}) copy-start(bf16[224,1024]{1,0:T(8,128)(2,1)S(1)} %get-tuple-element.32) | copy-start | bytes 1376260
  212.4 11.0 %copy-start.8 = (bf16[128,2048]{1,0:T(8,128)(2,1)S(1)}, bf16[128,2048]{1,0:T(8,128)(2,1)}, u32[]{:S(2)}) copy-start(bf16[128,2048]{1,0:T(8,128)(2,1)} %copy-done.7) | copy-start | bytes 1572868
  212.4 59.5 %collective-permute-start.8 = (bf16[224,512]{1,0:T(8,128)(2,1)}, bf16[224,512]{1,0:T(8,128)(2,1)}, u32[]{:S(2)}, u32[]{:S(2)}) collective-permute-start(bf16[224,512]{1,0:T(8,128)(2,1)} %get-tuple-element.28), channel_id=1, source_target_pairs={{0,8},{1,9},{2,10},{3,11},{4,12},{5,13},{6,14},{7,15},{8,16},{9,17... | collective-permute-start | bytes 688136 | tf_op jit(solution)/shard_map/ppermute | solution.py:118
  214.5 33.4 %collective-permute-start.5 = (bf16[256,2048]{1,0:T(8,128)(2,1)}, bf16[256,2048]{1,0:T(8,128)(2,1)S(1)}, u32[]{:S(2)}, u32[]{:S(2)}) collective-permute-start(bf16[256,2048]{1,0:T(8,128)(2,1)} %pad_maximum_fusion.2), channel_id=1, source_target_pairs={{0,24},{1,25},{2,26},{3,27},{4,28},{5,29},{6,30},{7,31},{8,0},{9,1... | collective-permute-start | bytes 3145736 | tf_op jit(solution)/shard_map/ppermute | solution.py:118
  249.5 4.1 %copy-start = (bf16[1,2048,224]{2,1,0:T(8,128)(2,1)}, bf16[1,2048,224]{2,1,0:T(8,128)(2,1)S(1)}, u32[]{:S(2)}) copy-start(bf16[1,2048,224]{2,1,0:T(8,128)(2,1)S(1)} %get-tuple-element.24) | copy-start | bytes 2752516
  258.5 18.0 %collective-permute-start.13 = (bf16[4,128,224]{1,0,2:T(4,128)(2,1)}, bf16[4,128,224]{1,0,2:T(4,128)(2,1)}, u32[]{:S(2)}, u32[]{:S(2)}) collective-permute-start(bf16[4,128,224]{1,0,2:T(4,128)(2,1)} %get-tuple-element.33), channel_id=1, source_target_pairs={{0,8},{1,9},{2,10},{3,11},{4,12},{5,13},{6,14},{7,15},{8,16},{9,17... | collective-permute-start | bytes 688136 | tf_op jit(solution)/shard_map/ppermute | solution.py:118
  263.0 16.8 %collective-permute-start.10 = (bf16[224,512]{1,0:T(8,128)(2,1)}, bf16[224,512]{1,0:T(8,128)(2,1)S(1)}, u32[]{:S(2)}, u32[]{:S(2)}) collective-permute-start(bf16[224,512]{1,0:T(8,128)(2,1)} %get-tuple-element.29), channel_id=1, source_target_pairs={{0,16},{1,17},{2,18},{3,19},{4,20},{5,21},{6,22},{7,23},{8,24},{9,... | collective-permute-start | bytes 688136 | tf_op jit(solution)/shard_map/ppermute | solution.py:118
  266.9 19.9 %collective-permute-start.12 = (bf16[224,512]{1,0:T(8,128)(2,1)}, bf16[224,512]{1,0:T(8,128)(2,1)S(1)}, u32[]{:S(2)}, u32[]{:S(2)}) collective-permute-start(bf16[224,512]{1,0:T(8,128)(2,1)} %get-tuple-element.30), channel_id=1, source_target_pairs={{0,24},{1,25},{2,26},{3,27},{4,28},{5,29},{6,30},{7,31},{8,0},{9,1... | collective-permute-start | bytes 688136 | tf_op jit(solution)/shard_map/ppermute | solution.py:118
  269.3 13.7 %collective-permute-start.14 = (bf16[4,128,224]{1,0,2:T(4,128)(2,1)}, bf16[4,128,224]{1,0,2:T(4,128)(2,1)S(1)}, u32[]{:S(2)}, u32[]{:S(2)}) collective-permute-start(bf16[4,128,224]{1,0,2:T(4,128)(2,1)} %get-tuple-element.33), channel_id=1, source_target_pairs={{0,16},{1,17},{2,18},{3,19},{4,20},{5,21},{6,22},{7,23},{8,24},{9,... | collective-permute-start | bytes 688136 | tf_op jit(solution)/shard_map/ppermute | solution.py:118
  271.9 14.8 %collective-permute-start.15 = (bf16[4,128,224]{1,0,2:T(4,128)(2,1)}, bf16[4,128,224]{1,0,2:T(4,128)(2,1)S(1)}, u32[]{:S(2)}, u32[]{:S(2)}) collective-permute-start(bf16[4,128,224]{1,0,2:T(4,128)(2,1)} %get-tuple-element.33), channel_id=1, source_target_pairs={{0,24},{1,25},{2,26},{3,27},{4,28},{5,29},{6,30},{7,31},{8,0},{9,1... | collective-permute-start | bytes 688136 | tf_op jit(solution)/shard_map/ppermute | solution.py:118
  276.5 13.9 %collective-permute-start.7 = (bf16[4,128,224]{1,0,2:T(4,128)(2,1)S(1)}, bf16[4,128,224]{1,0,2:T(4,128)(2,1)S(1)}, u32[]{:S(2)}, u32[]{:S(2)}) collective-permute-start(bf16[4,128,224]{1,0,2:T(4,128)(2,1)S(1)} %get-tuple-element.34), channel_id=1, source_target_pairs={{0,8},{1,9},{2,10},{3,11},{4,12},{5,13},{6,14},{7,15},{8,16},{9,17... | collective-permute-start | bytes 688136 | tf_op jit(solution)/shard_map/ppermute | solution.py:118
  278.4 8.7 %copy-start.5 = (bf16[224,1024]{1,0:T(8,128)(2,1)S(1)}, bf16[224,1024]{1,0:T(8,128)(2,1)}, u32[]{:S(2)}) copy-start(bf16[224,1024]{1,0:T(8,128)(2,1)} %copy-done.4) | copy-start | bytes 1376260
  279.9 11.8 %collective-permute-start.9 = (bf16[4,128,224]{1,0,2:T(4,128)(2,1)S(1)}, bf16[4,128,224]{1,0,2:T(4,128)(2,1)S(1)}, u32[]{:S(2)}, u32[]{:S(2)}) collective-permute-start(bf16[4,128,224]{1,0,2:T(4,128)(2,1)S(1)} %get-tuple-element.34), channel_id=1, source_target_pairs={{0,16},{1,17},{2,18},{3,19},{4,20},{5,21},{6,22},{7,23},{8,24},{9,... | collective-permute-start | bytes 688136 | tf_op jit(solution)/shard_map/ppermute | solution.py:118
  283.0 11.7 %collective-permute-start.11 = (bf16[4,128,224]{1,0,2:T(4,128)(2,1)S(1)}, bf16[4,128,224]{1,0,2:T(4,128)(2,1)S(1)}, u32[]{:S(2)}, u32[]{:S(2)}) collective-permute-start(bf16[4,128,224]{1,0,2:T(4,128)(2,1)S(1)} %get-tuple-element.34), channel_id=1, source_target_pairs={{0,24},{1,25},{2,26},{3,27},{4,28},{5,29},{6,30},{7,31},{8,0},{9,1... | collective-permute-start | bytes 688136 | tf_op jit(solution)/shard_map/ppermute | solution.py:118
  288.4 11.1 %collective-permute-start.16 = (bf16[4,128,512]{2,1,0:T(8,128)(2,1)S(1)}, bf16[4,128,512]{2,1,0:T(8,128)(2,1)S(1)}, u32[]{:S(2)}, u32[]{:S(2)}) collective-permute-start(bf16[4,128,512]{2,1,0:T(8,128)(2,1)S(1)} %bitcast.111), channel_id=1, source_target_pairs={{0,480},{1,33},{2,482},{3,35},{4,484},{5,37},{6,486},{7,39},{8,488... | collective-permute-start | bytes 1572872 | tf_op jit(solution)/shard_map/ppermute | solution.py:115
  299.8 12.0 %collective-permute-start.17 = (bf16[4,64,512]{2,1,0:T(8,128)(2,1)S(1)}, bf16[4,64,512]{2,1,0:T(8,128)(2,1)S(1)}, u32[]{:S(2)}, u32[]{:S(2)}) collective-permute-start(bf16[4,64,512]{2,1,0:T(8,128)(2,1)S(1)} %slice.59), channel_id=1, source_target_pairs={{0,448},{1,65},{2,450},{3,67},{4,452},{5,69},{6,454},{7,71},{8,456... | collective-permute-start | bytes 786440 | tf_op jit(solution)/shard_map/ppermute | solution.py:115
  311.9 27.9 %copy-start.11 = (f32[128,2]{0,1:T(2,128)S(1)}, f32[128,2]{0,1:T(2,128)}, u32[]{:S(2)}) copy-start(f32[128,2]{0,1:T(2,128)} %param.9) | copy-start | bytes 3076
  311.9 14.2 %collective-permute-start.18 = (bf16[4,32,512]{2,1,0:T(8,128)(2,1)S(1)}, bf16[4,32,512]{2,1,0:T(8,128)(2,1)S(1)}, u32[]{:S(2)}, u32[]{:S(2)}) collective-permute-start(bf16[4,32,512]{2,1,0:T(8,128)(2,1)S(1)} %slice.60), channel_id=1, source_target_pairs={{0,384},{1,129},{2,386},{3,131},{4,388},{5,133},{6,390},{7,135},{8... | collective-permute-start | bytes 393224 | tf_op jit(solution)/shard_map/ppermute | solution.py:115
  327.3 13.8 %copy-start.1 = (bf16[1,2048,224]{2,1,0:T(8,128)(2,1)S(1)}, bf16[1,2048,224]{2,1,0:T(8,128)(2,1)}, u32[]{:S(2)}) copy-start(bf16[1,2048,224]{2,1,0:T(8,128)(2,1)} %copy-done) | copy-start | bytes 2752516
  327.3 29.6 %all-to-all-start.3 = ((bf16[32,32,512]{2,1,0:T(8,128)(2,1)}), bf16[32,32,512]{2,1,0:T(8,128)(2,1)}, u32[]{:S(2)}, u32[]{:S(2)}) async-start(bf16[32,32,512]{2,1,0:T(8,128)(2,1)} %bitcast.106), calls=%async_computation.3 | async-start | bytes 2097152 | tf_op jit(solution)/shard_map/all_to_all | solution.py:204
